TPU v7x, 128 devices: a whole 4x4x4 slice. The times are simulated.
128 devices in a mesh: rep: 2 (over z_hi), fs: 32 (over z_lo, y, x), tp: 2 (over core).
Axes of the slice: x: 4, y: 4, z: 4 (z_hi: 2, z_lo: 2; z = z_hi * 2 + z_lo), core: 2. Of those that a mesh axis runs over, the one named last changes fastest.
Arguments:
- stream_in: bfloat16 [64, 768, 2048], P(('rep', 'fs'), None, 'tp'), may hold values from -6 to 6
- mix_gain: float32 [2048], replicated, may hold values from 0.1 to 1.9
- lin_weight: bfloat16 [2048, 2048], P('fs', 'tp'), may hold values from -0.125 to 0.125
- branch_weight: bfloat16 [2048, 2048], P('fs', 'tp'), may hold values from -0.125 to 0.125
- lin_taps: float32 [4, 2048], P(None, 'tp'), may hold values from -3 to 3
- rate_blocks: bfloat16 [16, 128, 128], P('tp'), may hold values from -0.5 to 0.5
- admit_blocks: bfloat16 [16, 128, 128], P('tp'), may hold values from -0.5 to 0.5
- decay_logit: float32 [2048], P('tp'), may hold values from 3.5 to 9
- mix_out_gain: float32 [2048], P('tp'), may hold values from 0.1 to 1.9
- out_weight: bfloat16 [2048, 2048], P('tp', 'fs'), may hold values from -0.125 to 0.125
- ffn_gain: float32 [2048], replicated, may hold values from 0.1 to 1.9
- gate_weight: bfloat16 [2048, 2816], P('fs', 'tp'), may hold values from -0.125 to 0.125
- up_weight: bfloat16 [2048, 2816], P('fs', 'tp'), may hold values from -0.125 to 0.125
- gate_taps: float32 [3, 2816], P(None, 'tp'), may hold values from -3 to 3
- up_taps: float32 [3, 2816], P(None, 'tp'), may hold values from -3 to 3
- down_weight: bfloat16 [2816, 2048], P('tp', 'fs'), may hold values from -0.109375 to 0.109375
Outputs:
- stream_out: bfloat16 [64, 768, 2048], P(('rep', 'fs'), None, 'tp')
All inputs are finite; a program needn't handle non-finite values.
Results may differ from a plain program's by a relative error of at most 0.018.
Values may be sent and summed in bfloat16 or wider, within the bound.
A program may use at most 128 MiB of HBM per device.

v0:
```python
import jax
import jax.numpy as jnp
from jax import lax
from jax.sharding import PartitionSpec as P

EPS = 1e-06
GATE_SCALE = 8.0


def sent_to_all(value, axis):
    count = lax.axis_size(axis)
    return lax.all_to_all(
        jnp.broadcast_to(value[None], (count, *value.shape)), axis, 0, 0, tiled=True
    )


def in_order(tiles, dim):
    tiles = jnp.moveaxis(tiles, 0, dim)
    dims = tiles.shape
    return tiles.reshape(*dims[:dim], dims[dim] * dims[dim + 1], *dims[dim + 2 :])


def collect(value, axis, dim):
    tiles = sent_to_all(value, axis)
    return in_order(tiles, dim)


def side_by_side(arrays, axis, dim, along):
    widths = [a.shape[along] for a in arrays]
    both = jnp.concatenate(arrays, axis=along)
    whole = lax.all_gather(both, axis, axis=dim, tiled=True)
    return tuple(jnp.split(whole, [sum(widths[:k]) for k in range(1, len(widths))], axis=along))


def split_up(value, dim, count):
    before, after = (value.shape[:dim], value.shape[dim + 1 :])
    return jnp.moveaxis(value.reshape(*before, count, -1, *after), dim, 0)


def sent_and_summed(value, axis, dim):
    count = lax.axis_size(axis)
    tiles = lax.all_to_all(split_up(value, dim, count), axis, 0, 0, tiled=True)
    return jnp.sum(tiles.astype(jnp.float32), axis=0)


def norm_rows(values, scales):
    mean_sq = jnp.mean(values * values, axis=-1, keepdims=True)
    return values * lax.rsqrt(mean_sq + EPS) * scales


def causal_filter(values, kernel):
    kernel_len = kernel.shape[0]
    seq_len = values.shape[0]
    padded = jnp.pad(values, ((kernel_len - 1, 0), (0, 0)))
    summed = padded[0:seq_len] * kernel[0]
    for offset in range(1, kernel_len):
        summed = summed + padded[offset : offset + seq_len] * kernel[offset]
    return summed


def chain_combine(earlier, later):
    return (earlier[0] * later[0], later[0] * earlier[1] + later[1])


def pair_folder(source, pieces):
    return (
        jnp.dot(source, pieces[0], preferred_element_type=jnp.float32),
        jnp.dot(source, pieces[1], preferred_element_type=jnp.float32),
    )


def local(
    stream_in,
    mix_gain,
    lin_weight,
    branch_weight,
    lin_taps,
    rate_blocks,
    admit_blocks,
    decay_logit,
    mix_out_gain,
    out_weight,
    ffn_gain,
    gate_weight,
    up_weight,
    gate_taps,
    up_taps,
    down_weight,
):
    own_rows = stream_in[0]
    length = own_rows.shape[0]
    full_rows = collect(own_rows, "tp", 1)
    normed = norm_rows(full_rows.astype(jnp.float32), mix_gain).astype(jnp.bfloat16)
    linear, branch = pair_folder(normed, side_by_side((lin_weight, branch_weight), "fs", 0, 1))
    linear = linear.astype(jnp.bfloat16)
    branch = branch.astype(jnp.bfloat16)
    filtered = causal_filter(linear.astype(jnp.float32), lin_taps)
    block_count = rate_blocks.shape[0]
    block_width = rate_blocks.shape[1]
    blocks = filtered.astype(jnp.bfloat16).reshape(length, block_count, block_width)
    rate_gate = jax.nn.sigmoid(
        jnp.einsum("lbi,bij->lbj", blocks, rate_blocks, preferred_element_type=jnp.float32).reshape(
            length, -1
        )
    )
    admitted = jax.nn.sigmoid(
        jnp.einsum(
            "lbi,bij->lbj", blocks, admit_blocks, preferred_element_type=jnp.float32
        ).reshape(length, -1)
    )
    log_decay = -GATE_SCALE * rate_gate * jax.nn.softplus(-decay_logit)
    decay = jnp.exp(log_decay)
    driven = jnp.sqrt(-jnp.expm1(2.0 * log_decay)) * admitted * filtered
    _, states = lax.associative_scan(chain_combine, (decay, driven), axis=0)
    gated = (states * jax.nn.gelu(branch.astype(jnp.float32))).reshape(
        length, block_count, block_width
    )
    gated = gated * lax.rsqrt(jnp.mean(gated * gated, axis=-1, keepdims=True) + EPS)
    mixed = (gated.reshape(length, -1) * mix_out_gain).astype(jnp.bfloat16)
    mix_partial = jnp.dot(
        mixed,
        lax.all_gather(out_weight, "fs", axis=1, tiled=True),
        preferred_element_type=jnp.float32,
    )
    my_share = sent_and_summed(mix_partial.astype(jnp.bfloat16), "tp", 1)
    middle_own = (own_rows.astype(jnp.float32) + my_share).astype(jnp.bfloat16)
    middle_full = collect(middle_own, "tp", 1)
    normed2 = norm_rows(middle_full.astype(jnp.float32), ffn_gain).astype(jnp.bfloat16)
    gate_pre, up_pre = pair_folder(normed2, side_by_side((gate_weight, up_weight), "fs", 0, 1))
    gate_pre = gate_pre.astype(jnp.bfloat16)
    up_pre = up_pre.astype(jnp.bfloat16)
    gate_conv = causal_filter(gate_pre.astype(jnp.float32), gate_taps)
    up_conv = causal_filter(up_pre.astype(jnp.float32), up_taps)
    hidden = (jax.nn.silu(gate_conv) * up_conv).astype(jnp.bfloat16)
    down_partial = jnp.dot(
        hidden,
        lax.all_gather(down_weight, "fs", axis=1, tiled=True),
        preferred_element_type=jnp.float32,
    )
    down_share = sent_and_summed(down_partial.astype(jnp.bfloat16), "tp", 1)
    result = (middle_own.astype(jnp.float32) + down_share).astype(jnp.bfloat16)
    return result[None]


def solution(mesh):
    placed = (
        P(("rep", "fs"), None, "tp"),
        P(),
        P("fs", "tp"),
        P("fs", "tp"),
        P(None, "tp"),
        P("tp", None, None),
        P("tp", None, None),
        P("tp"),
        P("tp"),
        P("tp", "fs"),
        P(),
        P("fs", "tp"),
        P("fs", "tp"),
        P(None, "tp"),
        P(None, "tp"),
        P("tp", "fs"),
    )
    return jax.shard_map(
        local, mesh=mesh, in_specs=placed, out_specs=P(("rep", "fs"), None, "tp"), check_vma=False
    )
```

profile of v0, /device:TPU:1, one launch (start us, length us, event | category | flops | bytes accessed | tf_op | source)
XLA Modules:
  0.0 707.7 jit_solution(17645392529465928909)
XLA Ops:
  14.5 5.3 all-to-all-start
  20.4 2.6 all-to-all-done
  24.5 2.4 fusion.3
  26.9 131.2 %all-gather.5.cloned.1.call-done = bf16[2048,2048]{1,0:T(8,128)(2,1)} async-done(((bf16[64,2048]{1,0:T(8,128)(2,1)}), bf16[2048,2048]{1,0:T(8,128)(2,1)}) %all-gather.5.cloned.1.call-update) | async-done | bytes 8388624 | tf_op jit(solution)/shard_map/all_gather | solution.py:31
  158.1 6.7 fusion.38
  164.8 3.1 convert_bitcast_fusion
  169.0 2.3 copy.66
  171.3 2.5 add_divide_fusion
  173.8 2.4 copy.67
  176.2 7.6 %multiply_exponential_fusion = (f32[768,1024]{1,0:T(8,128)}, f32[768,1024]{1,0:T(8,128)S(1)}) fusion(f32[768,1024]{1,0:T(8,128)} %copy.66, f32[1024]{0:T(1024)S(1)} %fusion.62, f32[768,1024]{1,0:T(8,128)} %get-tuple-element.14, f32[768,1024]{1,0:T(8,128)} %copy.67), kind=kLoop, calls=%fused_computation.51 | loop fusion | flops 3932160 | bytes 15732736 | tf_op jit(solution)/shard_map/exp | solution.py:112
  183.8 4.2 slice.277
  188.0 4.2 slice.278
  192.1 7.6 %slice.276 = f32[384,1024]{1,0:T(8,128)} slice(f32[768,1024]{1,0:T(8,128)} %get-tuple-element.15), slice={[1:768:2], [0:1024:1]} | slice | bytes 3145728 | tf_op jit(solution)/shard_map/slice | solution.py:114
  199.8 7.6 %slice.280 = f32[384,1024]{1,0:T(8,128)} slice(f32[768,1024]{1,0:T(8,128)} %get-tuple-element.15), slice={[0:767:2], [0:1024:1]} | slice | bytes 3145728 | tf_op jit(solution)/shard_map/slice | solution.py:114
  207.4 5.6 fusion.66
  213.0 4.3 slice.283
  217.3 4.3 slice.284
  221.6 4.3 slice.282
  225.9 4.3 slice.286
  230.3 3.4 fusion.67
  233.6 2.7 slice.289
  236.3 2.7 slice.290
  239.0 2.7 slice.288
  241.7 2.7 slice.292
  244.4 2.4 fusion.68
  290.0 2.7 slice.287
  292.8 2.7 slice.338
  296.9 4.4 slice.281
  301.3 4.4 slice.340
  307.0 4.4 slice.342
  311.4 7.9 %slice.275 = f32[383,1024]{1,0:T(8,128)} slice(f32[768,1024]{1,0:T(8,128)} %get-tuple-element.15), slice={[2:768:2], [0:1024:1]} | slice | bytes 3137536 | tf_op jit(solution)/shard_map/slice | solution.py:114
  331.2 2.3 pad.82
  334.9 9.6 %pad.84 = f32[768,1024]{1,0:T(8,128)} pad(f32[384,1024]{1,0:T(8,128)} %add.241, f32[]{:T(128)} %constant.11.clone.1), padding=1_0_1x0_0_0 | pad | bytes 4718596 | tf_op jit(solution)/shard_map/pad | solution.py:114
  344.5 2.6 fusion.47
  347.3 5.6 pad.83
  352.9 9.5 %fusion.29 = f32[768,1024]{1,0:T(8,128)S(1)} fusion(f32[768,1024]{1,0:T(8,128)} %pad.83, f32[768,1024]{1,0:T(8,128)} %pad.84, bf16[768,2048]{0,1:T(8,128)(2,1)} %fusion.3, bf16[2048,2048]{1,0:T(8,128)(2,1)} %all-gather.5.cloned.1.call-done), kind=kOutput, calls=%fused_computation.34 | convolution fusion | flops 3230662656 | bytes 16777216 | tf_op jit(solution)/shard_map/dot_general | solution.py:68
  370.6 6.2 convolution_convert_fusion
  377.2 27.0 %all_to_all.20 = bf16[2,768,1024]{2,1,0:T(8,128)(2,1)S(1)} all-to-all(bf16[2,768,1024]{2,1,0:T(8,128)(2,1)S(1)} %bitcast.82), channel_id=1, replica_groups=mesh['rep'=2,'fs'=32,'tp'=2] {'tp'}, dimensions={0} | all-to-all | bytes 6291456 | tf_op jit(solution)/shard_map/all_to_all | solution.py:42
  407.3 2.6 copy.62
  411.5 6.3 all_to_all.21
  418.5 2.5 fusion.1
  421.0 70.5 %all-gather.9.cloned.1.call-done = bf16[2048,2816]{1,0:T(8,128)(2,1)} async-done(((bf16[64,2816]{1,0:T(8,128)(2,1)}), bf16[2048,2816]{1,0:T(8,128)(2,1)}) %all-gather.9.cloned.1.call-update) | async-done | bytes 11534352 | tf_op jit(solution)/shard_map/all_gather | solution.py:31
  491.5 9.9 %fusion.15 = f32[768,1408]{1,0:T(8,128)} fusion(bf16[768,2048]{0,1:T(8,128)(2,1)} %fusion.1, bf16[2048,2816]{1,0:T(8,128)(2,1)} %all-gather.9.cloned.1.call-done), kind=kOutput, calls=%fused_computation.25 | convolution fusion | flops 4431347712 | bytes 13238272 | tf_op jit(solution)/shard_map/dot_general | solution.py:67
  501.5 6.7 fusion.21
  508.2 143.4 %all-gather.11.cloned.1.call-done = bf16[1408,2048]{0,1:T(8,128)(2,1)} async-done(((bf16[1408,64]{0,1:T(8,128)(2,1)}), bf16[1408,2048]{0,1:T(8,128)(2,1)}) %all-gather.11.cloned.1.call-update) | async-done | bytes 5767184 | tf_op jit(solution)/shard_map/all_gather | solution.py:137
  651.7 17.5 %convolution_convert_fusion.1 = bf16[768,2048]{1,0:T(8,128)(2,1)} fusion(bf16[1408,2048]{0,1:T(8,128)(2,1)} %all-gather.11.cloned.1.call-done, f32[768,1408]{1,0:T(8,128)} %fusion.21, f32[768,1408]{1,0:T(8,128)} %fusion.15, f32[1408]{0:T(1024)S(1)} %copy-done.26, f32[1408]{0:T(1024)S(1)} %copy-done.27, f32[1408]{0:T(1024)S(1)} %copy-done.25, ...), kind=kOutput, calls=%fused_computation.28 | convolution fusion | flops 4448059392 | bytes 17597440 | tf_op jit(solution)/shard_map/dot_general | solution.py:135
  669.2 2.3 copy.85
  671.5 26.0 %all_to_all.22 = bf16[2,768,1024]{2,1,0:T(8,128)(2,1)S(1)} all-to-all(bf16[2,768,1024]{2,1,0:T(8,128)(2,1)S(1)} %bitcast.83), channel_id=1, replica_groups=mesh['rep'=2,'fs'=32,'tp'=2] {'tp'}, dimensions={0} | all-to-all | bytes 6291456 | tf_op jit(solution)/shard_map/all_to_all | solution.py:42
  (186 shorter events, 87.5 us)
Async XLA Ops:
  6.5 161.3 %copy-start = (bf16[8,128,128]{2,1,0:T(8,128)(2,1)S(1)}, bf16[8,128,128]{2,1,0:T(8,128)(2,1)}, u32[]{:S(2)}) copy-start(bf16[8,128,128]{2,1,0:T(8,128)(2,1)} %param.21) | copy-start | bytes 786436
  6.5 151.6 %all-gather.5.cloned.1.call-start = ((), (), s32[]{:S(2)}) async-start(), calls=%async_computation.4 | async-start | bytes 8650752 | tf_op jit(solution)/shard_map/all_gather | solution.py:31
  8.3 360.4 %all-gather.7.cloned.1.call-start = ((), (), s32[]{:S(2)}) async-start(), calls=%async_computation.5 | async-start | bytes 4325376 | tf_op jit(solution)/shard_map/all_gather | solution.py:122
  9.0 482.5 %all-gather.9.cloned.1.call-start = ((), (), s32[]{:S(2)}) async-start(), calls=%async_computation.6 | async-start | bytes 11894784 | tf_op jit(solution)/shard_map/all_gather | solution.py:31
  14.5 8.6 %all-to-all-start = ((bf16[2,768,1024]{1,2,0:T(8,128)(2,1)}), bf16[2,768,1024]{1,2,0:T(8,128)(2,1)S(1)}, u32[]{:S(2)}, u32[]{:S(2)}) async-start(bf16[2,768,1024]{1,2,0:T(8,128)(2,1)} %broadcast_in_dim.9), calls=%async_computation | async-start | bytes 6291456 | tf_op jit(solution)/shard_map/all_to_all | solution.py:12
  19.8 4.0 copy-start.20
  19.8 4.0 copy-start.31
  19.8 4.0 copy-start.21
  19.8 4.0 copy-start.22
  19.8 4.7 copy-start.23
  19.8 631.8 %all-gather.11.cloned.1.call-start = ((), (), s32[]{:S(2)}) async-start(), calls=%async_computation.7 | async-start | bytes 5947392 | tf_op jit(solution)/shard_map/all_gather | solution.py:137
  167.8 1.1 copy-start.9
  169.0 2.3 copy-start.33
  307.0 12.9 %copy-start.11 = (f32[3,1024]{1,0:T(4,128)S(1)}, f32[3,1024]{1,0:T(4,128)}, u32[]{:S(2)}) copy-start(f32[3,1024]{1,0:T(4,128)} %slice.320) | copy-start | bytes 36868
  307.0 12.9 %copy-start.12 = (f32[3,1024]{1,0:T(4,128)S(1)}, f32[3,1024]{1,0:T(4,128)}, u32[]{:S(2)}) copy-start(f32[3,1024]{1,0:T(4,128)} %slice.318) | copy-start | bytes 36868
  307.0 12.9 %copy-start.13 = (f32[3,1024]{1,0:T(4,128)S(1)}, f32[3,1024]{1,0:T(4,128)}, u32[]{:S(2)}) copy-start(f32[3,1024]{1,0:T(4,128)} %slice.322) | copy-start | bytes 36868
  307.0 13.0 %copy-start.14 = (f32[2,1024]{1,0:T(2,128)S(1)}, f32[2,1024]{1,0:T(2,128)}, u32[]{:S(2)}) copy-start(f32[2,1024]{1,0:T(2,128)} %slice.317) | copy-start | bytes 24580
  307.0 13.0 %copy-start.15 = (f32[2,1024]{1,0:T(2,128)S(1)}, f32[2,1024]{1,0:T(2,128)}, u32[]{:S(2)}) copy-start(f32[2,1024]{1,0:T(2,128)} %slice.328) | copy-start | bytes 24580
  307.0 15.3 %copy-start.10 = (f32[11,1024]{1,0:T(8,128)S(1)}, f32[11,1024]{1,0:T(8,128)}, u32[]{:S(2)}) copy-start(f32[11,1024]{1,0:T(8,128)} %slice.332) | copy-start | bytes 135172
  319.9 6.0 copy-start.19
  326.0 1.7 copy-start.18
  326.3 4.3 copy-start.7
  326.3 4.3 copy-start.8
  329.6 1.3 copy-start.17
  344.5 2.6 copy-start.16
  362.4 1.7 copy-start.4
  364.8 5.7 copy-start.34
  366.5 4.1 copy-start.5
  404.2 1.4 copy-start.2
  417.8 0.7 copy-start.24
  491.5 9.9 %copy-start.6 = (bf16[768,2048]{0,1:T(8,128)(2,1)S(1)}, bf16[768,2048]{0,1:T(8,128)(2,1)}, u32[]{:S(2)}) copy-start(bf16[768,2048]{0,1:T(8,128)(2,1)} %fusion.1) | copy-start | bytes 9437188
  491.5 9.9 %copy-start.32 = (bf16[2048,2816]{1,0:T(8,128)(2,1)S(1)}, bf16[2048,2816]{1,0:T(8,128)(2,1)}, u32[]{:S(2)}) copy-start(bf16[2048,2816]{1,0:T(8,128)(2,1)} %all-gather.9.cloned.1.call-done) | copy-start | bytes 34603012
  501.4 150.2 %copy-start.25 = (f32[1408]{0:T(1024)S(1)}, f32[1408]{0:T(1024)}, u32[]{:S(2)}) copy-start(f32[1408]{0:T(1024)} %get-tuple-element.8) | copy-start | bytes 16900
  501.4 150.2 %copy-start.26 = (f32[1408]{0:T(1024)S(1)}, f32[1408]{0:T(1024)}, u32[]{:S(2)}) copy-start(f32[1408]{0:T(1024)} %get-tuple-element.9) | copy-start | bytes 16900
  501.5 150.2 %copy-start.27 = (f32[1408]{0:T(1024)S(1)}, f32[1408]{0:T(1024)}, u32[]{:S(2)}) copy-start(f32[1408]{0:T(1024)} %get-tuple-element.10) | copy-start | bytes 16900
  501.5 150.2 %copy-start.28 = (f32[1408]{0:T(1024)S(1)}, f32[1408]{0:T(1024)}, u32[]{:S(2)}) copy-start(f32[1408]{0:T(1024)} %get-tuple-element.38) | copy-start | bytes 16900
  501.5 150.2 %copy-start.29 = (f32[1408]{0:T(1024)S(1)}, f32[1408]{0:T(1024)}, u32[]{:S(2)}) copy-start(f32[1408]{0:T(1024)} %get-tuple-element.39) | copy-start | bytes 16900
  501.5 150.2 %copy-start.30 = (f32[1408]{0:T(1024)S(1)}, f32[1408]{0:T(1024)}, u32[]{:S(2)}) copy-start(f32[1408]{0:T(1024)} %get-tuple-element.40) | copy-start | bytes 16900
  697.4 1.4 copy-start.3
  697.4 3.5 copy-start.1
Sparse Core Ops, SparseCore 0:
  9.0 149.0 all-gather.4
  159.7 157.1 all-gather.6
  318.6 172.8 all-gather.8
  493.0 158.5 all-gather.10
where the time goes:
time: 714 us; the launch traced here: 708 us
  waiting for transfers between devices  349 us (49%)
  local copies, waits for them, and re-layouts  161 us (23%)
  matrix products  60.1 us (8%)
  blocking collectives  59.2 us (8%)
  other arithmetic  58.8 us (8%)
  between operations  14 us (2%)
    all_gather x2, waiting for transfers between devices, side_by_side(): whole = lax.all_gather(both, axis, axis=dim, tiled=True)  202 us
    all_gather x1, waiting for transfers between devices, local(): lax.all_gather(down_weight, 'fs', axis=1, tiled=True)  143 us
    slice x56, local copies, waits for them, and re-layouts, local(): _, states = lax.associative_scan(chain_combine, (decay, driven), axis=0)  118 us
    all_to_all x2, blocking collectives, sent_and_summed(): tiles = lax.all_to_all(split_up(value, dim, count), axis, 0, 0, tiled=True)  53 us
    pad x17, local copies, waits for them, and re-layouts, local(): _, states = lax.associative_scan(chain_combine, (decay, driven), axis=0)  19.3 us
    mul x8, other arithmetic, chain_combine(): return (earlier[0] * later[0], later[0] * earlier[1] + later[1])  17.9 us
    dot_general x1, matrix products, local(): jnp.dot(hidden, lax.all_gather(down_weight, 'fs', axis=1, tiled=True), pr...  17.5 us
    dot_general x2, matrix products, pair_folder(): jnp.dot(source, pieces[0], preferred_element_type=jnp.float32)  16.6 us
  transfers between devices with their start and end apart: 5, of which 4 were waited for; matrix products, arithmetic and copies ran while one was open for 36% of the time, Pallas kernels for 0%

commit v1 on v0

--- a/solution.py
+++ b/solution.py
@@ -134,7 +134,9 @@
     hidden = (jax.nn.silu(gate_conv) * up_conv).astype(jnp.bfloat16)
     down_partial = jnp.dot(
         hidden,
-        lax.all_gather(down_weight, "fs", axis=1, tiled=True),
+        jnp.concatenate(
+            lax.all_to_all(jnp.stack([down_weight] * lax.axis_size("fs")), "fs", 0, 0), axis=1
+        ),
         preferred_element_type=jnp.float32,
     )
     down_share = sent_and_summed(down_partial.astype(jnp.bfloat16), "tp", 1)

time: 714 us -> 638 us (0.89)
  waiting for transfers between devices: 349 us -> 250 us
  local copies, waits for them, and re-layouts: 161 us -> 174 us
    all_gather x1 -> x0, waiting for transfers between devices: 143 us -> none  [local(): lax.all_gather(down_weight, 'fs', axis=1, tiled=True)]
    all_gather x2, waiting for transfers between devices: 202 us -> 249 us  [side_by_side(): whole = lax.all_gather(both, axis, axis=dim, tiled=True)]
    slice x56, local copies, waits for them, and re-layouts: 118 us -> 130 us  [local(): _, states = lax.associative_scan(chain_combine, (decay, driven), axis=0)]
    all_to_all x1 -> x2, blocking collectives: 6.26 us -> 14.6 us  [sent_to_all(): lax.all_to_all(jnp.broadcast_to(value[None], (count, *value.shape)), axis...]
  transfers between devices with their start and end apart: 5 -> 4, of which waited for: 4 -> 2; matrix products, arithmetic and copies ran while one was open for 36% -> 42% of each run, Pallas kernels for 0% -> 0%
where the time goes in v1:
time: 638 us; the launch traced here: 625 us
  waiting for transfers between devices  250 us (39%)
  local copies, waits for them, and re-layouts  174 us (27%)
  blocking collectives  61.9 us (10%)
  other arithmetic  59.5 us (9%)
  matrix products  58.4 us (9%)
  between operations  14.1 us (2%)
  starting transfers between devices  7.52 us (1%)
    all_gather x2, waiting for transfers between devices, side_by_side(): whole = lax.all_gather(both, axis, axis=dim, tiled=True)  249 us
    slice x56, local copies, waits for them, and re-layouts, local(): _, states = lax.associative_scan(chain_combine, (decay, driven), axis=0)  130 us
    all_to_all x2, blocking collectives, sent_and_summed(): tiles = lax.all_to_all(split_up(value, dim, count), axis, 0, 0, tiled=True)  47.2 us
    pad x17, local copies, waits for them, and re-layouts, local(): _, states = lax.associative_scan(chain_combine, (decay, driven), axis=0)  19.5 us
    mul x8, other arithmetic, chain_combine(): return (earlier[0] * later[0], later[0] * earlier[1] + later[1])  17.9 us
    dot_general x1, matrix products, local(): jnp.dot(hidden, jnp.concatenate(lax.all_to_all(jnp.stack([down_weight] *...  17.5 us
    dot_general x2, matrix products, pair_folder(): jnp.dot(source, pieces[1], preferred_element_type=jnp.float32)  16.2 us
    dot_general x2, matrix products, pair_folder(): jnp.dot(source, pieces[0], preferred_element_type=jnp.float32)  15.1 us
  transfers between devices with their start and end apart: 4, of which 2 were waited for; matrix products, arithmetic and copies ran while one was open for 42% of the time, Pallas kernels for 0%

profile of v1, /device:TPU:1, one launch (start us, length us, event | category | flops | bytes accessed | tf_op | source)
XLA Modules:
  0.0 625.5 jit_solution(1235947694335623603)
XLA Ops:
  12.8 7.3 %all_to_all.25 = bf16[2,768,1024]{1,2,0:T(8,128)(2,1)S(1)} all-to-all(bf16[2,768,1024]{1,2,0:T(8,128)(2,1)S(1)} %broadcast_in_dim.9), channel_id=1, replica_groups=mesh['rep'=2,'fs'=32,'tp'=2] {'tp'}, dimensions={0} | all-to-all | bytes 6291456 | tf_op jit(solution)/shard_map/all_to_all | solution.py:12
  21.7 136.4 %all-gather.4.cloned.1.call-done = bf16[2048,2048]{1,0:T(8,128)(2,1)} async-done(((bf16[64,2048]{1,0:T(8,128)(2,1)}), bf16[2048,2048]{1,0:T(8,128)(2,1)}) %all-gather.4.cloned.1.call-update) | async-done | bytes 8388624 | tf_op jit(solution)/shard_map/all_gather | solution.py:31
  158.1 5.2 fusion.38
  163.4 3.1 convert_bitcast_fusion
  167.6 2.4 copy.67
  170.0 2.5 add_divide_fusion
  172.5 2.4 copy.68
  174.9 7.7 %multiply_exponential_fusion = (f32[768,1024]{1,0:T(8,128)}, f32[768,1024]{1,0:T(8,128)S(1)}) fusion(f32[768,1024]{1,0:T(8,128)} %copy.67, f32[1024]{0:T(1024)S(1)} %fusion.62, f32[768,1024]{1,0:T(8,128)} %get-tuple-element.14, f32[768,1024]{1,0:T(8,128)} %copy.68), kind=kLoop, calls=%fused_computation.51 | loop fusion | flops 3932160 | bytes 15732736 | tf_op jit(solution)/shard_map/exp | solution.py:112
  182.6 4.2 slice.277
  186.8 4.2 slice.278
  191.0 7.6 %slice.276 = f32[384,1024]{1,0:T(8,128)} slice(f32[768,1024]{1,0:T(8,128)} %get-tuple-element.15), slice={[1:768:2], [0:1024:1]} | slice | bytes 3145728 | tf_op jit(solution)/shard_map/slice | solution.py:114
  198.6 7.6 %slice.280 = f32[384,1024]{1,0:T(8,128)} slice(f32[768,1024]{1,0:T(8,128)} %get-tuple-element.15), slice={[0:767:2], [0:1024:1]} | slice | bytes 3145728 | tf_op jit(solution)/shard_map/slice | solution.py:114
  206.2 5.5 fusion.66
  211.7 4.3 slice.283
  216.0 4.3 slice.284
  220.4 4.3 slice.282
  224.7 4.3 slice.286
  229.0 3.4 fusion.67
  232.4 2.7 slice.289
  235.1 2.7 slice.290
  237.8 2.7 slice.288
  240.5 2.7 slice.292
  243.2 2.4 fusion.68
  250.6 13.2 %slice.298 = f32[48,1024]{1,0:T(8,128)} slice(f32[96,1024]{1,0:T(8,128)} %get-tuple-element.21), slice={[0:95:2], [0:1024:1]} | slice | bytes 393216 | tf_op jit(solution)/shard_map/slice | solution.py:114
  300.5 2.8 slice.287
  303.3 2.8 slice.338
  307.4 4.4 slice.340
  311.8 4.4 slice.281
  317.5 4.4 slice.342
  321.9 7.7 %slice.275 = f32[383,1024]{1,0:T(8,128)} slice(f32[768,1024]{1,0:T(8,128)} %get-tuple-element.15), slice={[2:768:2], [0:1024:1]} | slice | bytes 3137536 | tf_op jit(solution)/shard_map/slice | solution.py:114
  341.5 2.3 pad.82
  345.2 9.8 %pad.84 = f32[768,1024]{1,0:T(8,128)} pad(f32[384,1024]{1,0:T(8,128)} %add.241, f32[]{:T(128)} %constant.11.clone.1), padding=1_0_1x0_0_0 | pad | bytes 4718596 | tf_op jit(solution)/shard_map/pad | solution.py:114
  355.0 2.6 fusion.47
  357.7 5.7 pad.83
  363.4 9.5 %fusion.29 = f32[768,1024]{1,0:T(8,128)S(1)} fusion(f32[768,1024]{1,0:T(8,128)} %pad.83, f32[768,1024]{1,0:T(8,128)} %pad.84, bf16[768,2048]{0,1:T(8,128)(2,1)} %copy-done.7, bf16[2048,2048]{1,0:T(8,128)(2,1)} %all-gather.4.cloned.1.call-done), kind=kOutput, calls=%fused_computation.34 | convolution fusion | flops 3230662656 | bytes 16777216 | tf_op jit(solution)/shard_map/dot_general | solution.py:68
  381.1 6.0 convolution_convert_fusion
  387.5 26.9 %all_to_all.26 = bf16[2,768,1024]{2,1,0:T(8,128)(2,1)S(1)} all-to-all(bf16[2,768,1024]{2,1,0:T(8,128)(2,1)S(1)} %bitcast.85), channel_id=1, replica_groups=mesh['rep'=2,'fs'=32,'tp'=2] {'tp'}, dimensions={0} | all-to-all | bytes 6291456 | tf_op jit(solution)/shard_map/all_to_all | solution.py:42
  417.5 2.7 copy.63
  421.8 7.4 %all_to_all.27 = bf16[2,768,1024]{1,2,0:T(8,128)(2,1)} all-to-all(bf16[2,768,1024]{1,2,0:T(8,128)(2,1)S(1)} %broadcast_in_dim.11), channel_id=1, replica_groups=mesh['rep'=2,'fs'=32,'tp'=2] {'tp'}, dimensions={0} | all-to-all | bytes 6291456 | tf_op jit(solution)/shard_map/all_to_all | solution.py:12
  429.2 3.2 stack.2
  432.4 7.4 %all-to-all-start.3 = ((bf16[32,1408,64]{1,2,0:T(8,128)(2,1)}), bf16[32,1408,64]{1,2,0:T(8,128)(2,1)}, u32[]{:S(2)}, u32[]{:S(2)}) async-start(bf16[32,1408,64]{1,2,0:T(8,128)(2,1)} %stack.2), calls=%async_computation.3 | async-start | bytes 11534336 | tf_op jit(solution)/shard_map/all_to_all | solution.py:138
  440.0 2.8 multiply_reduce_fusion
  442.8 2.5 fusion.1
  445.3 113.0 %all-gather.8.cloned.1.call-done = bf16[2048,2816]{1,0:T(8,128)(2,1)} async-done(((bf16[64,2816]{1,0:T(8,128)(2,1)}), bf16[2048,2816]{1,0:T(8,128)(2,1)}) %all-gather.8.cloned.1.call-update) | async-done | bytes 11534352 | tf_op jit(solution)/shard_map/all_gather | solution.py:31
  558.4 9.9 %fusion.15 = f32[768,1408]{1,0:T(8,128)} fusion(bf16[768,2048]{0,1:T(8,128)(2,1)} %fusion.1, bf16[2048,2816]{1,0:T(8,128)(2,1)} %all-gather.8.cloned.1.call-done), kind=kOutput, calls=%fused_computation.25 | convolution fusion | flops 4431347712 | bytes 13238272 | tf_op jit(solution)/shard_map/dot_general | solution.py:67
  568.3 6.7 %fusion.21 = f32[768,1408]{1,0:T(8,128)} fusion(bf16[768,2048]{0,1:T(8,128)(2,1)S(1)} %copy-done.8, bf16[2048,2816]{1,0:T(8,128)(2,1)S(1)} %copy-done.29), kind=kOutput, calls=%fused_computation.27 | convolution fusion | flops 4431347712 | bytes 13238272 | tf_op jit(solution)/shard_map/dot_general | solution.py:68
  574.9 17.5 %convolution_convert_fusion.1 = bf16[768,2048]{1,0:T(8,128)(2,1)} fusion(bf16[1408,2048]{0,1:T(8,128)(2,1)} %bitcast.17, f32[768,1408]{1,0:T(8,128)} %fusion.21, f32[768,1408]{1,0:T(8,128)} %fusion.15, f32[1408]{0:T(1024)S(1)} %get-tuple-element.9, f32[1408]{0:T(1024)S(1)} %get-tuple-element.10, f32[1408]{0:T(1024)S(1)} %get-tuple-element.8, ...), kind=kOutput, calls=%fused_computation.28 | convolution fusion | flops 4448059392 | bytes 17597440 | tf_op jit(solution)/shard_map/dot_general | solution.py:135
  594.7 20.3 %all_to_all.28 = bf16[2,768,1024]{2,1,0:T(8,128)(2,1)S(1)} all-to-all(bf16[2,768,1024]{2,1,0:T(8,128)(2,1)S(1)} %bitcast.86), channel_id=1, replica_groups=mesh['rep'=2,'fs'=32,'tp'=2] {'tp'}, dimensions={0} | all-to-all | bytes 6291456 | tf_op jit(solution)/shard_map/all_to_all | solution.py:42
  (179 shorter events, 85.5 us)
Async XLA Ops:
  6.5 159.9 %copy-start = (bf16[8,128,128]{2,1,0:T(8,128)(2,1)S(1)}, bf16[8,128,128]{2,1,0:T(8,128)(2,1)}, u32[]{:S(2)}) copy-start(bf16[8,128,128]{2,1,0:T(8,128)(2,1)} %param.21) | copy-start | bytes 786436
  6.5 151.5 %all-gather.4.cloned.1.call-start = ((), (), s32[]{:S(2)}) async-start(), calls=%async_computation.5 | async-start | bytes 8650752 | tf_op jit(solution)/shard_map/all_gather | solution.py:31
  8.3 370.9 %all-gather.6.cloned.1.call-start = ((), (), s32[]{:S(2)}) async-start(), calls=%async_computation.6 | async-start | bytes 4325376 | tf_op jit(solution)/shard_map/all_gather | solution.py:122
  9.0 549.3 %all-gather.8.cloned.1.call-start = ((), (), s32[]{:S(2)}) async-start(), calls=%async_computation.7 | async-start | bytes 11894784 | tf_op jit(solution)/shard_map/all_gather | solution.py:31
  20.1 0.7 copy-start.28
  20.1 0.7 copy-start.23
  20.1 0.8 copy-start.26
  21.7 141.7 %copy-start.7 = (bf16[768,2048]{0,1:T(8,128)(2,1)}, bf16[768,2048]{0,1:T(8,128)(2,1)S(1)}, u32[]{:S(2)}) copy-start(bf16[768,2048]{0,1:T(8,128)(2,1)S(1)} %fusion.3) | copy-start | bytes 9437188
  166.4 1.1 copy-start.11
  167.6 2.4 copy-start.30
  317.5 12.7 %copy-start.14 = (f32[3,1024]{1,0:T(4,128)S(1)}, f32[3,1024]{1,0:T(4,128)}, u32[]{:S(2)}) copy-start(f32[3,1024]{1,0:T(4,128)} %slice.320) | copy-start | bytes 36868
  317.5 12.7 %copy-start.15 = (f32[3,1024]{1,0:T(4,128)S(1)}, f32[3,1024]{1,0:T(4,128)}, u32[]{:S(2)}) copy-start(f32[3,1024]{1,0:T(4,128)} %slice.318) | copy-start | bytes 36868
  317.5 12.7 %copy-start.16 = (f32[3,1024]{1,0:T(4,128)S(1)}, f32[3,1024]{1,0:T(4,128)}, u32[]{:S(2)}) copy-start(f32[3,1024]{1,0:T(4,128)} %slice.322) | copy-start | bytes 36868
  317.5 12.8 %copy-start.17 = (f32[2,1024]{1,0:T(2,128)S(1)}, f32[2,1024]{1,0:T(2,128)}, u32[]{:S(2)}) copy-start(f32[2,1024]{1,0:T(2,128)} %slice.317) | copy-start | bytes 24580
  317.5 12.8 %copy-start.18 = (f32[2,1024]{1,0:T(2,128)S(1)}, f32[2,1024]{1,0:T(2,128)}, u32[]{:S(2)}) copy-start(f32[2,1024]{1,0:T(2,128)} %slice.328) | copy-start | bytes 24580
  317.5 15.1 %copy-start.12 = (f32[11,1024]{1,0:T(8,128)S(1)}, f32[11,1024]{1,0:T(8,128)}, u32[]{:S(2)}) copy-start(f32[11,1024]{1,0:T(8,128)} %slice.332) | copy-start | bytes 135172
  330.2 6.0 copy-start.22
  336.2 1.7 copy-start.21
  336.6 4.3 copy-start.9
  336.6 4.3 copy-start.10
  339.9 1.3 copy-start.20
  354.9 2.6 copy-start.19
  372.9 1.7 copy-start.5
  375.3 5.7 copy-start.31
  376.9 4.1 copy-start.6
  414.4 1.4 copy-start.3
  421.8 7.4 %copy-start.13 = (bf16[1408,64]{0,1:T(8,128)(2,1)S(1)}, bf16[1408,64]{0,1:T(8,128)(2,1)}, u32[]{:S(2)}) copy-start(bf16[1408,64]{0,1:T(8,128)(2,1)} %param.31) | copy-start | bytes 540676
  432.4 7.5 %copy-start.24 = (f32[3,1408]{1,0:T(4,128)S(1)}, f32[3,1408]{1,0:T(4,128)}, u32[]{:S(2)}) copy-start(f32[3,1408]{1,0:T(4,128)} %param.30) | copy-start | bytes 50692
  432.4 7.5 %copy-start.25 = (f32[3,1408]{1,0:T(4,128)S(1)}, f32[3,1408]{1,0:T(4,128)}, u32[]{:S(2)}) copy-start(f32[3,1408]{1,0:T(4,128)} %param.29) | copy-start | bytes 50692
  432.4 142.5 %all-to-all-start.3 = ((bf16[32,1408,64]{1,2,0:T(8,128)(2,1)}), bf16[32,1408,64]{1,2,0:T(8,128)(2,1)}, u32[]{:S(2)}, u32[]{:S(2)}) async-start(bf16[32,1408,64]{1,2,0:T(8,128)(2,1)} %stack.2), calls=%async_computation.3 | async-start | bytes 11534336 | tf_op jit(solution)/shard_map/all_to_all | solution.py:138
  439.9 2.9 copy-start.2
  439.9 2.9 copy-start.27
  558.4 9.9 %copy-start.8 = (bf16[768,2048]{0,1:T(8,128)(2,1)S(1)}, bf16[768,2048]{0,1:T(8,128)(2,1)}, u32[]{:S(2)}) copy-start(bf16[768,2048]{0,1:T(8,128)(2,1)} %fusion.1) | copy-start | bytes 9437188
  558.4 9.9 %copy-start.29 = (bf16[2048,2816]{1,0:T(8,128)(2,1)S(1)}, bf16[2048,2816]{1,0:T(8,128)(2,1)}, u32[]{:S(2)}) copy-start(bf16[2048,2816]{1,0:T(8,128)(2,1)} %all-gather.8.cloned.1.call-done) | copy-start | bytes 34603012
  615.1 1.4 copy-start.4
  615.1 3.5 copy-start.1
Sparse Core Ops, SparseCore 0:
  9.0 149.0 all-gather.3
  159.7 157.1 all-gather.5
  318.6 239.7 all-gather.7
